TPU v7x, 32 devices: a whole 2x2x4 slice. The times are simulated.
32 devices in a mesh: ep: 16 (over z, y, x), tp: 2 (over core).
Axes of the slice: x: 2, y: 2, z: 4, core: 2. Of those that a mesh axis runs over, the one named last changes fastest.
Arguments:
- tokens: bfloat16 [256, 2048], P('ep'), may hold values from -6 to 6
- lengths: int32 [256], P('ep'), may hold values from 1 to 1024, as said below
- attn_gain: float32 [2048], replicated, may hold values from 0.1 to 1.9
- w_query: bfloat16 [2048, 1024], P(None, 'tp'), may hold values from -0.125 to 0.125
- w_key: bfloat16 [2048, 128], P(None, 'tp'), may hold values from -0.125 to 0.125
- w_value: bfloat16 [2048, 128], P(None, 'tp'), may hold values from -0.125 to 0.125
- head_bias: float32 [16], P('tp'), may hold values from -7 to -2
- key_cache: bfloat16 [256, 2, 64, 1024], P('ep', 'tp'), may hold values from -6 to 6
- value_cache: bfloat16 [256, 2, 64, 1024], P('ep', 'tp'), may hold values from -6 to 6
- w_attn_out: bfloat16 [1024, 2048], P('tp'), may hold values from -0.1875 to 0.1875
- ffn_gain: float32 [2048], replicated, may hold values from 0.1 to 1.9
- w_router: bfloat16 [2048, 16], replicated, may hold values from -0.125 to 0.125
- routes: int32 [256, 6], P('ep'), may hold values from 0 to 15, all different within a row; in each aligned block of 16 rows (0 to 15, 16 to 31, ...) at most 12 rows name the same one
- w_dense_gate: bfloat16 [2048, 512], P('ep', 'tp'), may hold values from -0.125 to 0.125
- w_dense_up: bfloat16 [2048, 512], P('ep', 'tp'), may hold values from -0.125 to 0.125
- w_dense_down: bfloat16 [512, 2048], P('tp', 'ep'), may hold values from -0.25 to 0.25
- dense_mix: float32 [2048], replicated, may hold values from -0.125 to 0.125
- w_expert_gate: bfloat16 [16, 2048, 512], P('ep', None, 'tp'), may hold values from -0.125 to 0.125
- w_expert_up: bfloat16 [16, 2048, 512], P('ep', None, 'tp'), may hold values from -0.125 to 0.125
- w_expert_down: bfloat16 [16, 512, 2048], P('ep', 'tp'), may hold values from -0.25 to 0.25
Outputs:
- layer_out: bfloat16 [256, 2048], P('ep', 'tp')
- new_keys: bfloat16 [256, 128], P('ep', 'tp')
- new_values: bfloat16 [256, 128], P('ep', 'tp')
Inputs may be any that keep to these rules, and one draw needn't show every extreme that they name: `lengths`: every sequence holds between 1 and 1024 cached positions; in every draw some sequence holds exactly 1024. `routes`: each token names 6 different experts. Among the rows of one device no expert is named by more than 12 rows.
All inputs are finite; a program needn't handle non-finite values.
Results may differ from a plain program's by a relative error of at most 0.014.
Values may be sent and summed in bfloat16 or wider, within the bound.
A program may use at most 64 MiB of HBM per device.

v0:
```python
import jax
import jax.numpy as jnp
from jax import lax
from jax.sharding import PartitionSpec as P


def rms_scale(values, gain):
    wide = values.astype(jnp.float32)
    return wide * lax.rsqrt(jnp.mean(wide * wide, axis=-1, keepdims=True) + 1e-06) * gain


def stick_read(queries, lengths, head_bias, key_cache, value_cache):
    seq_count, local_kv, head_dim, cache_len = key_cache.shape
    group_size = head_bias.shape[0] // local_kv
    grouped = queries.reshape(seq_count, local_kv, group_size, head_dim)
    head_shift = head_bias.reshape(1, local_kv, group_size, 1)
    span_len = min(512, cache_len)
    block_count = (jnp.max(lengths) + span_len - 1) // span_len
    span_index = lax.iota(jnp.int32, span_len)
    after_mask = (span_index[:, None] > span_index[None, :]).astype(jnp.float32)

    def visit(visit_index, carry):
        totals, log_later = carry
        first = (block_count - 1 - visit_index) * span_len
        key_block = lax.dynamic_slice_in_dim(key_cache, first, span_len, 3)
        value_block = lax.dynamic_slice_in_dim(value_cache, first, span_len, 3)
        scores = (
            jnp.einsum("skgd,skdc->skgc", grouped, key_block, preferred_element_type=jnp.float32)
            * head_dim ** (-0.5)
            + head_shift
        )
        positions = first + span_index
        visible = (positions[None, :] < lengths[:, None])[:, None, None, :]
        log_keep = jnp.where(visible, jax.nn.log_sigmoid(-scores), 0.0)
        log_after = (
            jnp.einsum("skgj,jc->skgc", log_keep, after_mask, precision=lax.Precision.HIGHEST)
            + log_later[..., None]
        )
        weights = jnp.where(visible, jnp.exp(jax.nn.log_sigmoid(scores) + log_after), 0.0).astype(
            jnp.bfloat16
        )
        totals = totals + jnp.einsum(
            "skgc,skdc->skgd", weights, value_block, preferred_element_type=jnp.float32
        )
        return (totals, log_later + jnp.sum(log_keep, axis=3))

    start_totals = jnp.zeros((seq_count, local_kv, group_size, head_dim), jnp.float32)
    start_later = jnp.zeros((seq_count, local_kv, group_size), jnp.float32)
    totals, unused_later = lax.fori_loop(0, block_count, visit, (start_totals, start_later))
    return totals.reshape(seq_count, -1).astype(jnp.bfloat16)


def expert_math(inputs, w_expert_gate, w_expert_up, w_expert_down):
    gate_rows = jnp.einsum(
        "njcd,jdf->njcf", inputs, w_expert_gate, preferred_element_type=jnp.float32
    )
    up_rows = jnp.einsum("njcd,jdf->njcf", inputs, w_expert_up, preferred_element_type=jnp.float32)
    hidden = (jax.nn.silu(gate_rows) * up_rows).astype(jnp.bfloat16)
    partial_value = jnp.einsum(
        "njcf,jfd->njcd", hidden, w_expert_down, preferred_element_type=jnp.float32
    ).astype(jnp.bfloat16)
    return (
        lax.psum_scatter(partial_value, "tp", scatter_dimension=3, tiled=True)
        .astype(jnp.float32)
        .astype(jnp.bfloat16)
    )


def shards(
    tokens,
    lengths,
    attn_gain,
    w_query,
    w_key,
    w_value,
    head_bias,
    key_cache,
    value_cache,
    w_attn_out,
    ffn_gain,
    w_router,
    routes,
    w_dense_gate,
    w_dense_up,
    w_dense_down,
    dense_mix,
    w_expert_gate,
    w_expert_up,
    w_expert_down,
):
    seq_count, model_width = tokens.shape
    normed = rms_scale(tokens, attn_gain).astype(jnp.bfloat16)
    new_keys = jnp.dot(normed, w_key, preferred_element_type=jnp.float32).astype(jnp.bfloat16)
    new_values = jnp.dot(normed, w_value, preferred_element_type=jnp.float32).astype(jnp.bfloat16)
    queries = jnp.dot(normed, w_query, preferred_element_type=jnp.float32).astype(jnp.bfloat16)
    heads_out = stick_read(queries, lengths, head_bias, key_cache, value_cache)
    attn_partial = jnp.dot(heads_out, w_attn_out, preferred_element_type=jnp.float32).astype(
        jnp.bfloat16
    )
    attn = lax.psum(attn_partial, "tp").astype(jnp.float32)
    residual = (tokens.astype(jnp.float32) + attn).astype(jnp.bfloat16)
    normed2 = rms_scale(residual, ffn_gain).astype(jnp.bfloat16)
    expert_total = w_router.shape[1]
    top_count = routes.shape[1]
    probs = jax.nn.sigmoid(jnp.dot(normed2, w_router, preferred_element_type=jnp.float32))
    hits = routes[:, :, None] == lax.iota(jnp.int32, expert_total)[None, None, :]
    picked = jnp.sum(jnp.where(hits, probs[:, None, :], 0.0), axis=-1)
    gates = picked / jnp.sum(picked, axis=-1, keepdims=True) * 2.5
    capacity = max(2, 2 * seq_count * top_count // expert_total)
    slot_total = expert_total * capacity
    flat_routes = routes.reshape(-1)
    route_count = flat_routes.shape[0]
    matching = flat_routes[:, None] == flat_routes[None, :]
    earlier = lax.iota(jnp.int32, route_count)[:, None] > lax.iota(jnp.int32, route_count)[None, :]
    slot_rank = jnp.sum(jnp.logical_and(matching, earlier).astype(jnp.int32), axis=1)
    target = flat_routes * capacity + slot_rank
    one_hot = (target[:, None] == lax.iota(jnp.int32, slot_total)[None, :]).astype(jnp.bfloat16)
    dispatch = jnp.sum(one_hot.reshape(seq_count, top_count, slot_total), axis=1)
    send_rows = jnp.einsum(
        "sr,sd->rd", dispatch, normed2, preferred_element_type=jnp.float32
    ).astype(jnp.bfloat16)
    send_rows = send_rows.reshape(expert_total, capacity, model_width)
    local_experts = w_expert_gate.shape[0]
    received = lax.all_to_all(send_rows, "ep", split_axis=0, concat_axis=0, tiled=True)
    source_count = received.shape[0] // local_experts
    item_count = received.shape[1]
    inputs = received.reshape(source_count, local_experts, item_count, model_width)
    summed = expert_math(inputs, w_expert_gate, w_expert_up, w_expert_down)
    summed = summed.reshape(source_count * local_experts, item_count, summed.shape[3])
    returned = lax.all_to_all(summed, "ep", split_axis=0, concat_axis=0, tiled=True)
    half_width = returned.shape[2]
    route_rows = returned.reshape(slot_total, half_width)[target]
    route_rows = route_rows.reshape(seq_count, top_count, half_width)
    routed = jnp.sum(gates[:, :, None] * route_rows.astype(jnp.float32), axis=1)
    features2 = lax.all_to_all(normed2, "ep", split_axis=1, concat_axis=0, tiled=True)
    paired_weights = jnp.concatenate([w_dense_gate, w_dense_up], axis=1)
    paired = lax.psum_scatter(
        jnp.dot(features2, paired_weights, preferred_element_type=jnp.float32),
        "ep",
        scatter_dimension=0,
        tiled=True,
    )
    hidden_cols = w_dense_gate.shape[1]
    dense_gate_rows = paired[:, :hidden_cols]
    dense_up_rows = paired[:, hidden_cols:]
    dense_hidden = (jax.nn.silu(dense_gate_rows) * dense_up_rows).astype(jnp.bfloat16)
    dense_columns = jnp.dot(
        lax.all_gather(dense_hidden, "ep", axis=0, tiled=True),
        w_dense_down,
        preferred_element_type=jnp.float32,
    )
    dense_partial = lax.all_to_all(
        dense_columns.astype(jnp.bfloat16), "ep", split_axis=0, concat_axis=1, tiled=True
    )
    dense = lax.psum_scatter(dense_partial, "tp", scatter_dimension=1, tiled=True).astype(
        jnp.float32
    )
    mix_gate = jax.nn.sigmoid(jnp.sum(normed2.astype(jnp.float32) * dense_mix, axis=-1))
    offset = lax.axis_index("tp") * half_width
    residual_half = lax.dynamic_slice_in_dim(residual, offset, half_width, 1)
    layer_out = (residual_half.astype(jnp.float32) + mix_gate[:, None] * dense + routed).astype(
        jnp.bfloat16
    )
    return (layer_out, new_keys, new_values)


def solution(mesh):
    return jax.shard_map(
        shards,
        mesh=mesh,
        in_specs=(
            P("ep", None),
            P("ep"),
            P(),
            P(None, "tp"),
            P(None, "tp"),
            P(None, "tp"),
            P("tp"),
            P("ep", "tp", None, None),
            P("ep", "tp", None, None),
            P("tp", None),
            P(),
            P(),
            P("ep", None),
            P("ep", "tp"),
            P("ep", "tp"),
            P("tp", "ep"),
            P(),
            P("ep", None, "tp"),
            P("ep", None, "tp"),
            P("ep", "tp", None),
        ),
        out_specs=(P("ep", "tp"), P("ep", "tp"), P("ep", "tp")),
        check_vma=False,
    )
```

profile of v0, /device:TPU:0, one launch (start us, length us, event | category | flops | bytes accessed | tf_op | source)
XLA Modules:
  0.0 217.0 jit_solution(16179048854171437925)
XLA Ops:
  7.2 1.4 reduce_max.9
  9.3 1.0 fusion.40
  10.3 2.1 convolution_convert_fusion.4
  12.4 0.1 reshape.238
  12.5 3.9 %while.15 = (s32[]{:T(128)}, f32[16,1,8,64]{3,2,0,1:T(8,128)S(1)}, f32[16,1,8]{0,2,1:T(8,128)S(1)}, s32[]{:T(128)}, s32[]{:T(128)}, /*index=5*/s32[16]{0:T(128)S...) while((s32[]{:T(128)}, f32[16,1,8,64]{3,2,0,1:T(8,128)S(1)}, ...), condition=%wide.region_4.5_spmd.clone, body=%wide.region_2.4_spmd.clone.sunk | while | flops 422003200 | bytes 11420487 | solution.py:49
  12.7 1.6 fusion.88
  14.4 0.9 fusion.89
  15.3 0.7 copy-done.1
  16.0 0.4 fusion.90
  16.5 0.1 convert_element_type.104
  16.6 1.0 convolution_convert_fusion.2
  17.7 0.1 eq.45
  17.8 0.2 convert_reduce_fusion
  18.2 0.1 fusion.50
  18.3 23.8 %all-reduce.2.cloned.1.call-done = bf16[16,2048]{1,0:T(8,128)(2,1)} async-done(((bf16[16,2048]{1,0:T(8,128)(2,1)}), bf16[16,2048]{1,0:T(8,128)(2,1)}) %all-reduce.2.cloned.1.call-update) | async-done | bytes 65552 | tf_op jit(solution)/shard_map/psum | solution.py:100
  42.1 1.0 fusion.37
  43.1 0.2 multiply_reduce_fusion.1
  43.3 0.6 copy.71
  43.9 6.8 %all-to-all-start = ((bf16[16,16,128]{2,0,1:T(8,128)(2,1)}), bf16[16,16,128]{2,0,1:T(8,128)(2,1)S(1)}, u32[]{:S(2)}, u32[]{:S(2)}) async-start(bf16[16,16,128]{2,0,1:T(8,128)(2,1)} %bitcast.105), calls=%async_computation | async-start | bytes 131072 | tf_op jit(solution)/shard_map/all_to_all | solution.py:135
  50.8 0.4 convolution_convert_fusion.1
  51.2 1.2 reshape.240
  52.3 5.9 %all-to-all-done = bf16[16,16,128]{2,0,1:T(8,128)(2,1)S(1)} async-done(((bf16[16,16,128]{2,0,1:T(8,128)(2,1)}), bf16[16,16,128]{2,0,1:T(8,128)(2,1)S(1)}, u32[]{:S(2)}, u32[]{:S(2)}) %all-to-all-start) | async-done | bytes 65568 | tf_op jit(solution)/shard_map/all_to_all | solution.py:135
  58.3 3.7 %all-to-all-start.2 = ((bf16[16,12,2048]{2,1,0:T(8,128)(2,1)}), bf16[16,12,2048]{2,1,0:T(8,128)(2,1)S(1)}, u32[]{:S(2)}, u32[]{:S(2)}) async-start(bf16[16,12,2048]{2,1,0:T(8,128)(2,1)} %reshape.240), calls=%async_computation.4 | async-start | bytes 2097152 | tf_op jit(solution)/shard_map/all_to_all | solution.py:124
  62.0 1.0 fusion.44
  63.1 0.1 mul.144
  63.2 23.2 %all-to-all-done.2 = bf16[16,12,2048]{2,1,0:T(8,128)(2,1)S(1)} async-done(((bf16[16,12,2048]{2,1,0:T(8,128)(2,1)}), bf16[16,12,2048]{2,1,0:T(8,128)(2,1)S(1)}, u32[]{:S(2)}, u32[]{:S(2)}) %all-to-all-start.2) | async-done | bytes 786464 | tf_op jit(solution)/shard_map/all_to_all | solution.py:124
  86.4 1.7 convolution_bitcast_fusion.2
  88.2 0.4 fusion.30
  88.7 0.8 copy-done.2
  89.5 1.3 fusion.27
  90.8 0.8 convolution_convert_fusion.5
  91.6 0.8 convolution_convert_fusion.6
  92.5 51.5 %reduce-scatter.4.cloned.1.call-done = f32[16,512]{1,0:T(8,128)} async-done(((f32[256,512]{1,0:T(8,128)}), f32[16,512]{1,0:T(8,128)}) %reduce-scatter.4.cloned.1.call-update) | async-done | bytes 32784 | tf_op jit(solution)/shard_map/reduce_scatter | solution.py:137
  144.0 0.7 fusion.52
  144.7 37.0 %all_gather.3 = bf16[256,256]{1,0:T(8,128)(2,1)S(1)} all-gather(bf16[16,256]{1,0:T(8,128)(2,1)S(1)} %fusion.52), channel_id=1, replica_groups=mesh['ep'=16,'tp'=2] {'ep'}, dimensions={0}, use_global_device_ids=true | all-gather | bytes 139264 | tf_op jit(solution)/shard_map/all_gather | solution.py:148
  181.7 0.8 convolution_convert_fusion.3
  182.5 3.5 %all-to-all-start.1 = ((bf16[16,16,128]{2,1,0:T(8,128)(2,1)}), bf16[16,16,128]{2,1,0:T(8,128)(2,1)S(1)}, u32[]{:S(2)}, u32[]{:S(2)}) async-start(bf16[16,16,128]{2,1,0:T(8,128)(2,1)} %bitcast.5), calls=%async_computation.2 | async-start | bytes 131072 | tf_op jit(solution)/shard_map/all_to_all | solution.py:152
  186.0 0.2 fusion.33
  186.2 0.2 select_reduce_fusion
  186.5 2.0 copy.64
  188.5 5.0 %all-to-all-done.1 = bf16[16,16,128]{2,1,0:T(8,128)(2,1)S(1)} async-done(((bf16[16,16,128]{2,1,0:T(8,128)(2,1)}), bf16[16,16,128]{2,1,0:T(8,128)(2,1)S(1)}, u32[]{:S(2)}, u32[]{:S(2)}) %all-to-all-start.1) | async-done | bytes 65568 | tf_op jit(solution)/shard_map/all_to_all | solution.py:152
  193.5 3.6 %all-to-all-start.3 = ((bf16[16,12,1024]{2,1,0:T(8,128)(2,1)}), bf16[16,12,1024]{2,1,0:T(8,128)(2,1)S(1)}, u32[]{:S(2)}, u32[]{:S(2)}) async-start(bf16[16,12,1024]{2,1,0:T(8,128)(2,1)} %copy.64), calls=%async_computation.6 | async-start | bytes 1048576 | tf_op jit(solution)/shard_map/all_to_all | solution.py:130
  197.2 0.6 copy_bitcast_fusion
  197.9 9.9 %all-to-all-done.3 = bf16[16,12,1024]{2,1,0:T(8,128)(2,1)S(1)} async-done(((bf16[16,12,1024]{2,1,0:T(8,128)(2,1)}), bf16[16,12,1024]{2,1,0:T(8,128)(2,1)S(1)}, u32[]{:S(2)}, u32[]{:S(2)}) %all-to-all-start.3) | async-done | bytes 393248 | tf_op jit(solution)/shard_map/all_to_all | solution.py:130
  207.8 0.1 reshape.246
  207.9 0.8 gather_fusion
  208.7 0.2 multiply_reduce_fusion
  209.0 1.5 add_convert_fusion
  (62 shorter events, 1.0 us)
Async XLA Ops:
  7.2 9.4 %copy-start = (bf16[512,2048]{1,0:T(8,128)(2,1)S(1)}, bf16[512,2048]{1,0:T(8,128)(2,1)}, u32[]{:S(2)}) copy-start(bf16[512,2048]{1,0:T(8,128)(2,1)} %param.31) | copy-start | bytes 6291460
  7.2 5.3 %copy-start.9 = (s32[16]{0:T(128)S(1)}, s32[16]{0:T(128)}, u32[]{:S(2)}) copy-start(s32[16]{0:T(128)} %param.23) | copy-start | bytes 196
  7.2 5.3 %copy-start.16 = (f32[8]{0:T(128)S(1)}, f32[8]{0:T(128)}, u32[]{:S(2)}) copy-start(f32[8]{0:T(128)} %param.28) | copy-start | bytes 100
  7.2 34.9 %all-reduce.2.cloned.1.call-start = ((), (), s32[]{:S(2)}) async-start(), calls=%async_computation.7 | async-start | bytes 131072 | tf_op jit(solution)/shard_map/psum | solution.py:100
  14.4 1.6 copy-start.1
  16.4 1.2 copy-start.8
  16.4 25.7 %copy-start.3 = (bf16[16,2048]{1,0:T(8,128)(2,1)S(1)}, bf16[16,2048]{1,0:T(8,128)(2,1)}, u32[]{:S(2)}) copy-start(bf16[16,2048]{1,0:T(8,128)(2,1)} %param.22) | copy-start | bytes 196612
  16.4 26.6 %copy-start.7 = (f32[2048]{0:T(1024)S(1)}, f32[2048]{0:T(1024)}, u32[]{:S(2)}) copy-start(f32[2048]{0:T(1024)} %param.32) | copy-start | bytes 24580
  16.4 26.6 %copy-start.11 = (f32[2048]{0:T(1024)S(1)}, f32[2048]{0:T(1024)}, u32[]{:S(2)}) copy-start(f32[2048]{0:T(1024)} %param.38) | copy-start | bytes 24580
  43.9 14.4 %all-to-all-start = ((bf16[16,16,128]{2,0,1:T(8,128)(2,1)}), bf16[16,16,128]{2,0,1:T(8,128)(2,1)S(1)}, u32[]{:S(2)}, u32[]{:S(2)}) async-start(bf16[16,16,128]{2,0,1:T(8,128)(2,1)} %bitcast.105), calls=%async_computation | async-start | bytes 131072 | tf_op jit(solution)/shard_map/all_to_all | solution.py:135
  51.2 10.8 %copy-start.5 = (bf16[128,256]{1,0:T(8,128)(2,1)S(1)}, bf16[128,256]{1,0:T(8,128)(2,1)}, u32[]{:S(2)}) copy-start(bf16[128,256]{1,0:T(8,128)(2,1)} %param.36) | copy-start | bytes 196612
  51.2 10.8 %copy-start.6 = (bf16[128,256]{1,0:T(8,128)(2,1)S(1)}, bf16[128,256]{1,0:T(8,128)(2,1)}, u32[]{:S(2)}) copy-start(bf16[128,256]{1,0:T(8,128)(2,1)} %param.35) | copy-start | bytes 196612
  58.3 28.1 %all-to-all-start.2 = ((bf16[16,12,2048]{2,1,0:T(8,128)(2,1)}), bf16[16,12,2048]{2,1,0:T(8,128)(2,1)S(1)}, u32[]{:S(2)}, u32[]{:S(2)}) async-start(bf16[16,12,2048]{2,1,0:T(8,128)(2,1)} %reshape.240), calls=%async_computation.4 | async-start | bytes 2097152 | tf_op jit(solution)/shard_map/all_to_all | solution.py:124
  62.0 82.0 %reduce-scatter.4.cloned.1.call-start = ((), (), s32[]{:S(2)}) async-start(), calls=%async_computation.8 | async-start | bytes 557056 | tf_op jit(solution)/shard_map/reduce_scatter | solution.py:137
  63.1 123.4 %reduce-scatter.8.cloned.1.call-start = ((), (), s32[]{:S(2)}) async-start(), calls=%async_computation.10 | async-start | bytes 1179648 | tf_op jit(solution)/shard_map/reduce_scatter | solution.py:63
  86.4 1.8 copy-start.12
  88.2 1.2 copy-start.2
  89.4 1.3 copy-start.10
  89.4 1.3 copy-start.13
  89.4 2.2 %copy-start.14 = (bf16[2048,64]{0,1:T(8,128)(2,1)S(1)}, bf16[2048,64]{0,1:T(8,128)(2,1)}, u32[]{:S(2)}) copy-start(bf16[2048,64]{0,1:T(8,128)(2,1)} %param.26) | copy-start | bytes 786436
  89.5 92.3 %copy-start.4 = (bf16[256,128]{1,0:T(8,128)(2,1)S(1)}, bf16[256,128]{1,0:T(8,128)(2,1)}, u32[]{:S(2)}) copy-start(bf16[256,128]{1,0:T(8,128)(2,1)} %param.37) | copy-start | bytes 196612
  89.5 96.5 %copy-start.15 = (bf16[2048,16]{0,1:T(8,128)(2,1)S(1)}, bf16[2048,16]{0,1:T(8,128)(2,1)}, u32[]{:S(2)}) copy-start(bf16[2048,16]{0,1:T(8,128)(2,1)} %param.33) | copy-start | bytes 196612
  182.5 11.0 %all-to-all-start.1 = ((bf16[16,16,128]{2,1,0:T(8,128)(2,1)}), bf16[16,16,128]{2,1,0:T(8,128)(2,1)S(1)}, u32[]{:S(2)}, u32[]{:S(2)}) async-start(bf16[16,16,128]{2,1,0:T(8,128)(2,1)} %bitcast.5), calls=%async_computation.2 | async-start | bytes 131072 | tf_op jit(solution)/shard_map/all_to_all | solution.py:152
  193.5 14.3 %all-to-all-start.3 = ((bf16[16,12,1024]{2,1,0:T(8,128)(2,1)}), bf16[16,12,1024]{2,1,0:T(8,128)(2,1)S(1)}, u32[]{:S(2)}, u32[]{:S(2)}) async-start(bf16[16,12,1024]{2,1,0:T(8,128)(2,1)} %copy.64), calls=%async_computation.6 | async-start | bytes 1048576 | tf_op jit(solution)/shard_map/all_to_all | solution.py:130
  197.1 11.9 %reduce-scatter.6.cloned.1.call-start = ((), (), s32[]{:S(2)}) async-start(), calls=%async_computation.9 | async-start | bytes 98304 | tf_op jit(solution)/shard_map/reduce_scatter | solution.py:155
Sparse Core Ops, SparseCore 0:
  17.7 24.2 all-reduce.1
  65.0 78.8 reduce-scatter.3
  146.2 4.7 reduce-scatter.7
  199.8 8.7 reduce-scatter.5
where the time goes:
time: 218 us; the launch traced here: 217 us
  waiting for transfers between devices  119 us (55%)
  blocking collectives  37 us (17%)
  starting transfers between devices  17.7 us (8%)
  between operations  14.8 us (7%)
  matrix products  13.6 us (6%)
  local copies, waits for them, and re-layouts  7.75 us (4%)
  other arithmetic  6.66 us (3%)
    reduce_scatter x1, waiting for transfers between devices, shards(): lax.psum_scatter(jnp.dot(features2, paired_weights, preferred_element_typ...  51.5 us
    all_gather x1, blocking collectives, shards(): lax.all_gather(dense_hidden, 'ep', axis=0, tiled=True)  37 us
    psum x1, waiting for transfers between devices, shards(): attn = lax.psum(attn_partial, 'tp').astype(jnp.float32)  23.8 us
    all_to_all x1, waiting for transfers between devices, shards(): lax.all_to_all(send_rows, 'ep', split_axis=0, concat_axis=0, tiled=True)  23.2 us
    all_to_all x1, waiting for transfers between devices, shards(): lax.all_to_all(summed, 'ep', split_axis=0, concat_axis=0, tiled=True)  9.93 us
    all_to_all x1, starting transfers between devices, shards(): lax.all_to_all(normed2, 'ep', split_axis=1, concat_axis=0, tiled=True)  6.83 us
    all_to_all x1, waiting for transfers between devices, shards(): lax.all_to_all(normed2, 'ep', split_axis=1, concat_axis=0, tiled=True)  5.95 us
    all_to_all x1, waiting for transfers between devices, shards(): lax.all_to_all(dense_columns.astype(jnp.bfloat16), 'ep', split_axis=0, co...  5.01 us
  transfers between devices with their start and end apart: 8, of which 6 were waited for; matrix products, arithmetic and copies ran while one was open for 7% of the time, Pallas kernels for 0%

commit v1 on v0

--- a/solution.py
+++ b/solution.py
@@ -132,7 +132,9 @@
     route_rows = returned.reshape(slot_total, half_width)[target]
     route_rows = route_rows.reshape(seq_count, top_count, half_width)
     routed = jnp.sum(gates[:, :, None] * route_rows.astype(jnp.float32), axis=1)
-    features2 = lax.all_to_all(normed2, "ep", split_axis=1, concat_axis=0, tiled=True)
+    cells = jnp.split(normed2, lax.axis_size("ep"), axis=1)
+    incoming = lax.all_to_all(jnp.stack(cells), "ep", 0, 0)
+    features2 = jnp.concatenate(incoming, axis=0)
     paired_weights = jnp.concatenate([w_dense_gate, w_dense_up], axis=1)
     paired = lax.psum_scatter(
         jnp.dot(features2, paired_weights, preferred_element_type=jnp.float32),

time: 218 us -> 226 us (1.037)
  local copies, waits for them, and re-layouts: 7.75 us -> 16.4 us
    unnamed x33 -> x54, local copies, waits for them, and re-layouts: 0.95 us -> 10.4 us
  transfers between devices with their start and end apart: 8 -> 8, of which waited for: 6 -> 6; matrix products, arithmetic and copies ran while one was open for 7% -> 6% of each run, Pallas kernels for 0% -> 0%
where the time goes in v1:
time: 226 us; the launch traced here: 225 us
  waiting for transfers between devices  118 us (52%)
  blocking collectives  37 us (16%)
  starting transfers between devices  17.7 us (8%)
  local copies, waits for them, and re-layouts  16.4 us (7%)
  between operations  14.8 us (7%)
  matrix products  13.7 us (6%)
  other arithmetic  7.17 us (3%)
    reduce_scatter x1, waiting for transfers between devices, shards(): lax.psum_scatter(jnp.dot(features2, paired_weights, preferred_element_typ...  51.4 us
    all_gather x1, blocking collectives, shards(): lax.all_gather(dense_hidden, 'ep', axis=0, tiled=True)  37 us
    all_to_all x1, waiting for transfers between devices, shards(): lax.all_to_all(send_rows, 'ep', split_axis=0, concat_axis=0, tiled=True)  23.2 us
    psum x1, waiting for transfers between devices, shards(): attn = lax.psum(attn_partial, 'tp').astype(jnp.float32)  22.8 us
    unnamed x54, local copies, waits for them, and re-layouts  10.4 us
    all_to_all x1, waiting for transfers between devices, shards(): lax.all_to_all(summed, 'ep', split_axis=0, concat_axis=0, tiled=True)  9.92 us
    all_to_all x1, starting transfers between devices, shards(): incoming = lax.all_to_all(jnp.stack(cells), 'ep', 0, 0)  6.83 us
    all_to_all x1, waiting for transfers between devices, shards(): incoming = lax.all_to_all(jnp.stack(cells), 'ep', 0, 0)  5.97 us
  transfers between devices with their start and end apart: 8, of which 6 were waited for; matrix products, arithmetic and copies ran while one was open for 6% of the time, Pallas kernels for 0%

profile of v1, /device:TPU:0, one launch (start us, length us, event | category | flops | bytes accessed | tf_op | source)
XLA Modules:
  0.0 225.4 jit_solution(12497826899775524569)
XLA Ops:
  7.2 1.4 reduce_max.9
  9.3 1.0 fusion.40
  10.3 2.1 convolution_convert_fusion.4
  12.5 3.4 %while.15 = (s32[]{:T(128)}, f32[16,1,8,64]{3,2,0,1:T(8,128)S(1)}, f32[16,1,8]{0,2,1:T(8,128)S(1)}, s32[]{:T(128)}, s32[]{:T(128)}, /*index=5*/s32[16]{0:T(128)S...) while((s32[]{:T(128)}, f32[16,1,8,64]{3,2,0,1:T(8,128)S(1)}, ...), condition=%wide.region_4.5_spmd.clone, body=%wide.region_2.4_spmd.clone.sunk | while | flops 422003200 | bytes 11420495 | solution.py:49
  12.7 1.8 fusion.88
  14.5 0.9 fusion.89
  16.1 1.0 convolution_convert_fusion.2
  18.3 22.8 %all-reduce.2.cloned.1.call-done = bf16[16,2048]{1,0:T(8,128)(2,1)} async-done(((bf16[16,2048]{1,0:T(8,128)(2,1)}), bf16[16,2048]{1,0:T(8,128)(2,1)}) %all-reduce.2.cloned.1.call-update) | async-done | bytes 65552 | tf_op jit(solution)/shard_map/psum | solution.py:100
  41.1 1.0 fusion.37
  42.1 0.7 multiply_reduce_fusion.1
  42.8 0.6 constant_dynamic-update-slice_fusion.15
  43.4 0.6 constant_dynamic-update-slice_fusion.14
  44.6 0.6 constant_dynamic-update-slice_fusion.12
  45.2 0.6 constant_dynamic-update-slice_fusion.11
  45.8 0.6 constant_dynamic-update-slice_fusion.10
  46.4 0.6 constant_dynamic-update-slice_fusion.9
  47.0 0.6 constant_dynamic-update-slice_fusion.8
  47.6 0.6 constant_dynamic-update-slice_fusion.7
  48.1 0.6 constant_dynamic-update-slice_fusion.6
  48.7 0.6 constant_dynamic-update-slice_fusion.5
  49.3 0.6 constant_dynamic-update-slice_fusion.4
  49.9 0.6 constant_dynamic-update-slice_fusion.3
  50.5 0.6 constant_dynamic-update-slice_fusion.2
  51.1 0.6 constant_dynamic-update-slice_fusion.1
  51.7 0.6 constant_dynamic-update-slice_fusion
  52.3 6.8 %all-to-all-start = ((bf16[16,16,128]{2,1,0:T(8,128)(2,1)}), bf16[16,16,128]{2,1,0:T(8,128)(2,1)S(1)}, u32[]{:S(2)}, u32[]{:S(2)}) async-start(bf16[16,16,128]{2,1,0:T(8,128)(2,1)} %constant_dynamic-update-slice_fusion), calls=%async_computation | async-start | bytes 131072 | tf_op jit(solution)/shard_map/all_to_all | solution.py:136
  59.5 1.1 reshape.241
  60.7 6.0 %all-to-all-done = bf16[16,16,128]{2,1,0:T(8,128)(2,1)S(1)} async-done(((bf16[16,16,128]{2,1,0:T(8,128)(2,1)}), bf16[16,16,128]{2,1,0:T(8,128)(2,1)S(1)}, u32[]{:S(2)}, u32[]{:S(2)}) %all-to-all-start) | async-done | bytes 65568 | tf_op jit(solution)/shard_map/all_to_all | solution.py:136
  66.7 3.7 %all-to-all-start.2 = ((bf16[16,12,2048]{2,1,0:T(8,128)(2,1)}), bf16[16,12,2048]{2,1,0:T(8,128)(2,1)S(1)}, u32[]{:S(2)}, u32[]{:S(2)}) async-start(bf16[16,12,2048]{2,1,0:T(8,128)(2,1)} %reshape.241), calls=%async_computation.4 | async-start | bytes 2097152 | tf_op jit(solution)/shard_map/all_to_all | solution.py:124
  70.4 1.0 fusion.44
  71.6 23.2 %all-to-all-done.2 = bf16[16,12,2048]{2,1,0:T(8,128)(2,1)S(1)} async-done(((bf16[16,12,2048]{2,1,0:T(8,128)(2,1)}), bf16[16,12,2048]{2,1,0:T(8,128)(2,1)S(1)}, u32[]{:S(2)}, u32[]{:S(2)}) %all-to-all-start.2) | async-done | bytes 786464 | tf_op jit(solution)/shard_map/all_to_all | solution.py:124
  94.8 1.7 convolution_bitcast_fusion.2
  97.0 0.8 copy-done.2
  97.8 1.3 fusion.27
  99.2 0.8 convolution_convert_fusion.6
  100.1 0.8 convolution_convert_fusion.5
  100.9 51.4 %reduce-scatter.4.cloned.1.call-done = f32[16,512]{1,0:T(8,128)} async-done(((f32[256,512]{1,0:T(8,128)}), f32[16,512]{1,0:T(8,128)}) %reduce-scatter.4.cloned.1.call-update) | async-done | bytes 32784 | tf_op jit(solution)/shard_map/reduce_scatter | solution.py:139
  152.3 0.7 fusion.52
  153.1 37.0 %all_gather.3 = bf16[256,256]{1,0:T(8,128)(2,1)S(1)} all-gather(bf16[16,256]{1,0:T(8,128)(2,1)S(1)} %fusion.52), channel_id=1, replica_groups=mesh['ep'=16,'tp'=2] {'ep'}, dimensions={0}, use_global_device_ids=true | all-gather | bytes 139264 | tf_op jit(solution)/shard_map/all_gather | solution.py:150
  190.1 0.8 convolution_convert_fusion.3
  190.9 3.5 %all-to-all-start.1 = ((bf16[16,16,128]{2,1,0:T(8,128)(2,1)}), bf16[16,16,128]{2,1,0:T(8,128)(2,1)S(1)}, u32[]{:S(2)}, u32[]{:S(2)}) async-start(bf16[16,16,128]{2,1,0:T(8,128)(2,1)} %bitcast.20), calls=%async_computation.2 | async-start | bytes 131072 | tf_op jit(solution)/shard_map/all_to_all | solution.py:154
  194.8 2.0 copy.61
  196.8 5.1 %all-to-all-done.1 = bf16[16,16,128]{2,1,0:T(8,128)(2,1)S(1)} async-done(((bf16[16,16,128]{2,1,0:T(8,128)(2,1)}), bf16[16,16,128]{2,1,0:T(8,128)(2,1)S(1)}, u32[]{:S(2)}, u32[]{:S(2)}) %all-to-all-start.1) | async-done | bytes 65568 | tf_op jit(solution)/shard_map/all_to_all | solution.py:154
  201.9 3.6 %all-to-all-start.3 = ((bf16[16,12,1024]{2,1,0:T(8,128)(2,1)}), bf16[16,12,1024]{2,1,0:T(8,128)(2,1)S(1)}, u32[]{:S(2)}, u32[]{:S(2)}) async-start(bf16[16,12,1024]{2,1,0:T(8,128)(2,1)} %copy.61), calls=%async_computation.6 | async-start | bytes 1048576 | tf_op jit(solution)/shard_map/all_to_all | solution.py:130
  205.6 0.6 copy_bitcast_fusion
  206.3 9.9 %all-to-all-done.3 = bf16[16,12,1024]{2,1,0:T(8,128)(2,1)S(1)} async-done(((bf16[16,12,1024]{2,1,0:T(8,128)(2,1)}), bf16[16,12,1024]{2,1,0:T(8,128)(2,1)S(1)}, u32[]{:S(2)}, u32[]{:S(2)}) %all-to-all-start.3) | async-done | bytes 393248 | tf_op jit(solution)/shard_map/all_to_all | solution.py:130
  216.3 0.8 gather_fusion
  217.4 1.5 add_convert_fusion
  (83 shorter events, 4.7 us)
Async XLA Ops:
  7.2 8.9 %copy-start = (bf16[512,2048]{1,0:T(8,128)(2,1)S(1)}, bf16[512,2048]{1,0:T(8,128)(2,1)}, u32[]{:S(2)}) copy-start(bf16[512,2048]{1,0:T(8,128)(2,1)} %param.31) | copy-start | bytes 6291460
  7.2 5.3 %copy-start.8 = (s32[16]{0:T(128)S(1)}, s32[16]{0:T(128)}, u32[]{:S(2)}) copy-start(s32[16]{0:T(128)} %param.23) | copy-start | bytes 196
  7.2 5.3 %copy-start.19 = (f32[8]{0:T(128)S(1)}, f32[8]{0:T(128)}, u32[]{:S(2)}) copy-start(f32[8]{0:T(128)} %param.28) | copy-start | bytes 100
  7.2 33.9 %all-reduce.2.cloned.1.call-start = ((), (), s32[]{:S(2)}) async-start(), calls=%async_computation.7 | async-start | bytes 131072 | tf_op jit(solution)/shard_map/psum | solution.py:100
  12.7 2.7 %copy-start.1 = (bf16[16,1,64,1024]{3,2,0,1:T(8,128)(2,1)S(1)}, bf16[16,1,64,1024]{3,2,0,1:T(8,128)(2,1)}, u32[]{:S(2)}) copy-start(bf16[16,1,64,1024]{3,2,0,1:T(8,128)(2,1)} %get-tuple-element.336) | copy-start | bytes 6291460 | tf_op jit(solution)/shard_map/while
  15.9 1.2 copy-start.7
  15.9 25.2 %copy-start.3 = (bf16[16,2048]{1,0:T(8,128)(2,1)S(1)}, bf16[16,2048]{1,0:T(8,128)(2,1)}, u32[]{:S(2)}) copy-start(bf16[16,2048]{1,0:T(8,128)(2,1)} %param.22) | copy-start | bytes 196612
  15.9 26.2 %copy-start.10 = (f32[2048]{0:T(1024)S(1)}, f32[2048]{0:T(1024)}, u32[]{:S(2)}) copy-start(f32[2048]{0:T(1024)} %param.38) | copy-start | bytes 24580
  16.0 26.1 %copy-start.11 = (f32[2048]{0:T(1024)S(1)}, f32[2048]{0:T(1024)}, u32[]{:S(2)}) copy-start(f32[2048]{0:T(1024)} %param.32) | copy-start | bytes 24580
  17.5 0.5 copy-start.13
  52.3 14.4 %all-to-all-start = ((bf16[16,16,128]{2,1,0:T(8,128)(2,1)}), bf16[16,16,128]{2,1,0:T(8,128)(2,1)S(1)}, u32[]{:S(2)}, u32[]{:S(2)}) async-start(bf16[16,16,128]{2,1,0:T(8,128)(2,1)} %constant_dynamic-update-slice_fusion), calls=%async_computation | async-start | bytes 131072 | tf_op jit(solution)/shard_map/all_to_all | solution.py:136
  59.5 10.9 %copy-start.5 = (bf16[128,256]{1,0:T(8,128)(2,1)S(1)}, bf16[128,256]{1,0:T(8,128)(2,1)}, u32[]{:S(2)}) copy-start(bf16[128,256]{1,0:T(8,128)(2,1)} %param.36) | copy-start | bytes 196612
  59.5 10.9 %copy-start.6 = (bf16[128,256]{1,0:T(8,128)(2,1)S(1)}, bf16[128,256]{1,0:T(8,128)(2,1)}, u32[]{:S(2)}) copy-start(bf16[128,256]{1,0:T(8,128)(2,1)} %param.35) | copy-start | bytes 196612
  66.7 28.1 %all-to-all-start.2 = ((bf16[16,12,2048]{2,1,0:T(8,128)(2,1)}), bf16[16,12,2048]{2,1,0:T(8,128)(2,1)S(1)}, u32[]{:S(2)}, u32[]{:S(2)}) async-start(bf16[16,12,2048]{2,1,0:T(8,128)(2,1)} %reshape.241), calls=%async_computation.4 | async-start | bytes 2097152 | tf_op jit(solution)/shard_map/all_to_all | solution.py:124
  70.3 82.0 %reduce-scatter.4.cloned.1.call-start = ((), (), s32[]{:S(2)}) async-start(), calls=%async_computation.8 | async-start | bytes 557056 | tf_op jit(solution)/shard_map/reduce_scatter | solution.py:139
  71.4 123.3 %reduce-scatter.8.cloned.1.call-start = ((), (), s32[]{:S(2)}) async-start(), calls=%async_computation.10 | async-start | bytes 1179648 | tf_op jit(solution)/shard_map/reduce_scatter | solution.py:63
  94.8 1.8 copy-start.15
  96.6 1.2 copy-start.2
  97.8 1.3 copy-start.14
  97.8 1.4 copy-start.9
  97.8 1.4 copy-start.16
  97.8 2.2 copy-start.17
  97.8 92.2 %copy-start.4 = (bf16[256,128]{1,0:T(8,128)(2,1)S(1)}, bf16[256,128]{1,0:T(8,128)(2,1)}, u32[]{:S(2)}) copy-start(bf16[256,128]{1,0:T(8,128)(2,1)} %param.37) | copy-start | bytes 196612
  97.8 96.5 %copy-start.18 = (bf16[2048,16]{0,1:T(8,128)(2,1)S(1)}, bf16[2048,16]{0,1:T(8,128)(2,1)}, u32[]{:S(2)}) copy-start(bf16[2048,16]{0,1:T(8,128)(2,1)} %param.33) | copy-start | bytes 196612
  99.1 106.5 %copy-start.12 = (f32[16]{0:T(128)S(1)}, f32[16]{0:T(128)}, u32[]{:S(2)}) copy-start(f32[16]{0:T(128)} %get-tuple-element.225) | copy-start | bytes 196
  190.9 11.0 %all-to-all-start.1 = ((bf16[16,16,128]{2,1,0:T(8,128)(2,1)}), bf16[16,16,128]{2,1,0:T(8,128)(2,1)S(1)}, u32[]{:S(2)}, u32[]{:S(2)}) async-start(bf16[16,16,128]{2,1,0:T(8,128)(2,1)} %bitcast.20), calls=%async_computation.2 | async-start | bytes 131072 | tf_op jit(solution)/shard_map/all_to_all | solution.py:154
  201.9 14.3 %all-to-all-start.3 = ((bf16[16,12,1024]{2,1,0:T(8,128)(2,1)}), bf16[16,12,1024]{2,1,0:T(8,128)(2,1)S(1)}, u32[]{:S(2)}, u32[]{:S(2)}) async-start(bf16[16,12,1024]{2,1,0:T(8,128)(2,1)} %copy.61), calls=%async_computation.6 | async-start | bytes 1048576 | tf_op jit(solution)/shard_map/all_to_all | solution.py:130
  205.4 11.9 %reduce-scatter.6.cloned.1.call-start = ((), (), s32[]{:S(2)}) async-start(), calls=%async_computation.9 | async-start | bytes 98304 | tf_op jit(solution)/shard_map/reduce_scatter | solution.py:157
Sparse Core Ops, SparseCore 0:
  17.3 23.7 all-reduce.1
  73.4 78.8 reduce-scatter.3
  154.6 4.7 reduce-scatter.7
  208.1 8.7 reduce-scatter.5
